TPU v7x, 32 devices: a whole 2x2x4 slice. The times are simulated.
32 devices in a mesh: ep: 4 (over y, x), tp: 8 (over z, core).
Axes of the slice: x: 2, y: 2, z: 4, core: 2. Of those that a mesh axis runs over, the one named last changes fastest.
Arguments:
- tokens: bfloat16 [256, 4096], P('ep'), may hold values from -6 to 6
- norm_gain: float32 [4096], replicated, may hold values from 0.1 to 1.9
- ffn_gain: float32 [4096], replicated, may hold values from 0.1 to 1.9
- w_in: bfloat16 [4096, 2048], P(None, 'tp'), may hold values from -0.09375 to 0.09375
- decay_rate: float32 [8192], P('tp'), may hold values from 0.02 to 2
- frequency: float32 [8192], P('tp'), may hold values from -3.140625 to 3.140625
- log_step: float32 [128], P('tp'), may hold values from -2.3 to 0
- input_real: float32 [16, 8192], P(None, 'tp'), may hold values from -1 to 1
- input_imag: float32 [16, 8192], P(None, 'tp'), may hold values from -1 to 1
- readout_real: float32 [16, 8192], P(None, 'tp'), may hold values from -0.5 to 0.5
- readout_imag: float32 [16, 8192], P(None, 'tp'), may hold values from -0.5 to 0.5
- skip_gain: float32 [2048], P('tp'), may hold values from -4 to 4
- state_real: float32 [256, 8192], P('ep', 'tp'), may hold values from -6 to 6
- state_imag: float32 [256, 8192], P('ep', 'tp'), may hold values from -6 to 6
- w_out: bfloat16 [2048, 4096], P('tp'), may hold values from -0.125 to 0.125
- shared_gate: bfloat16 [4096, 1024], P(None, 'tp'), may hold values from -0.09375 to 0.09375
- shared_up: bfloat16 [4096, 1024], P(None, 'tp'), may hold values from -0.09375 to 0.09375
- shared_down: bfloat16 [1024, 4096], P('tp'), may hold values from -0.1875 to 0.1875
- expert_gate: bfloat16 [16, 4096, 1024], P('ep', 'tp'), may hold values from -0.09375 to 0.09375
- expert_up: bfloat16 [16, 4096, 1024], P('ep', 'tp'), may hold values from -0.09375 to 0.09375
- expert_down: bfloat16 [16, 1024, 4096], P('ep', None, 'tp'), may hold values from -0.1875 to 0.1875
- routing: int32 [256, 4], P('ep'), may hold values from 0 to 15, all different within a row; in each aligned block of 64 rows (0 to 63, 64 to 127, ...) at most 32 rows name the same one
- route_weight: float32 [256, 4], P('ep'), may hold values from 0.1 to 1
Outputs:
- mixed: bfloat16 [256, 4096], P('ep', 'tp')
- new_state_real: float32 [256, 8192], P('ep', 'tp')
- new_state_imag: float32 [256, 8192], P('ep', 'tp')
Inputs may be any that keep to these rules, and one draw needn't show every extreme that they name: `routing`: each row names 4 different experts. In the rows of one index of ep (aligned blocks of 64 rows) no expert is named more than 32 times, and in every draw some expert is named exactly 32 times in some block.
All inputs are finite; a program needn't handle non-finite values.
Results may differ from a plain program's by a relative error of at most 0.02.
Values may be sent and summed in bfloat16 or wider, within the bound.
A program may use at most 64 MiB of HBM per device.

v0:
```python
import jax
import jax.numpy as jnp
from jax import lax
from jax.sharding import PartitionSpec as P

EPS = 1e-06
ROUTED_SCALE = 2.5
HIGH = lax.Precision.HIGHEST


def rms_scale(values_in, gains):
    values = values_in.astype(jnp.float32)
    factor = lax.rsqrt(jnp.mean(values * values, axis=-1, keepdims=True) + EPS)
    return (values * factor * gains).astype(jnp.bfloat16)


def state_update(
    normed,
    w_in,
    decay_rate,
    frequency,
    log_step,
    input_real,
    input_imag,
    readout_real,
    readout_imag,
    skip_gain,
    state_real,
    state_imag,
):
    seq_count = normed.shape[0]
    groups = log_step.shape[0]
    chan_count = skip_gain.shape[0] // groups
    state_width = decay_rate.shape[0] // groups
    drive_rows = jnp.dot(normed, w_in, preferred_element_type=jnp.float32).astype(jnp.bfloat16)
    drive_f = drive_rows.astype(jnp.float32).reshape(seq_count, groups, chan_count)
    decays = decay_rate.reshape(groups, state_width)
    omegas = frequency.reshape(groups, state_width)
    step_size = jnp.exp(log_step)[:, None]
    pole_mag = jnp.exp(-decays * step_size)
    pole_angle = omegas * step_size
    pole_re = pole_mag * jnp.cos(pole_angle)
    pole_im = pole_mag * jnp.sin(pole_angle)
    pole_norm = decays * decays + omegas * omegas
    diff_re = pole_re - 1.0
    lift_re = (-decays * diff_re + omegas * pole_im) / pole_norm
    lift_im = (-decays * pole_im - omegas * diff_re) / pole_norm
    in_re = input_real.reshape(chan_count, groups, state_width)
    in_im = input_imag.reshape(chan_count, groups, state_width)
    push_re = jnp.einsum("sgh,hgp->sgp", drive_f, in_re, precision=HIGH)
    push_im = jnp.einsum("sgh,hgp->sgp", drive_f, in_im, precision=HIGH)
    old_re = state_real.reshape(seq_count, groups, state_width)
    old_im = state_imag.reshape(seq_count, groups, state_width)
    new_re = pole_re * old_re - pole_im * old_im + lift_re * push_re - lift_im * push_im
    new_im = pole_re * old_im + pole_im * old_re + lift_re * push_im + lift_im * push_re
    out_re = readout_real.reshape(chan_count, groups, state_width)
    out_im = readout_imag.reshape(chan_count, groups, state_width)
    read_rows = jnp.einsum("sgp,hgp->sgh", new_re, out_re, precision=HIGH) - jnp.einsum(
        "sgp,hgp->sgh", new_im, out_im, precision=HIGH
    )
    read_rows = read_rows + skip_gain.reshape(groups, chan_count) * drive_f
    activated = jax.nn.gelu(read_rows).reshape(seq_count, groups * chan_count).astype(jnp.bfloat16)
    return (
        activated,
        new_re.reshape(seq_count, groups * state_width),
        new_im.reshape(seq_count, groups * state_width),
    )


def local(
    tokens,
    norm_gain,
    ffn_gain,
    w_in,
    decay_rate,
    frequency,
    log_step,
    input_real,
    input_imag,
    readout_real,
    readout_imag,
    skip_gain,
    state_real,
    state_imag,
    w_out,
    shared_gate,
    shared_up,
    shared_down,
    expert_gate,
    expert_up,
    expert_down,
    routing,
    route_weight,
):
    seq_count, model_width = tokens.shape
    tp_count = lax.axis_size("tp")
    ep_count = lax.axis_size("ep")
    slice_width = model_width // tp_count
    offset = lax.axis_index("tp") * slice_width
    normed = rms_scale(tokens, norm_gain)
    activated, new_real, new_imag = state_update(
        normed,
        w_in,
        decay_rate,
        frequency,
        log_step,
        input_real,
        input_imag,
        readout_real,
        readout_imag,
        skip_gain,
        state_real,
        state_imag,
    )
    mixer_terms = jnp.dot(activated, w_out, preferred_element_type=jnp.float32)
    mixer_own = lax.psum_scatter(mixer_terms, "tp", scatter_dimension=1, tiled=True)
    own_tokens = lax.dynamic_slice_in_dim(tokens, offset, slice_width, 1)
    resid_own = (own_tokens.astype(jnp.float32) + mixer_own).astype(jnp.bfloat16)
    resid_f = resid_own.astype(jnp.float32)
    square_sum = lax.psum(jnp.sum(resid_f * resid_f, axis=1, keepdims=True), "tp")
    factor = lax.rsqrt(square_sum / model_width + EPS)
    gain_own = lax.dynamic_slice_in_dim(ffn_gain, offset, slice_width, 0)
    rows_own = (resid_f * factor * gain_own).astype(jnp.bfloat16)
    ffn_rows = lax.all_gather(rows_own, "tp", axis=1, tiled=True)
    expert_dev = expert_gate.shape[0]
    expert_count = expert_dev * ep_count
    top_count = routing.shape[1]
    capacity = 2 * seq_count * top_count // expert_count
    slot_count = expert_count * capacity
    flat_ids = routing.reshape(-1)
    one_hot = (flat_ids[:, None] == jnp.arange(expert_count, dtype=jnp.int32)[None, :]).astype(
        jnp.int32
    )
    earlier = jnp.cumsum(one_hot, axis=0) - one_hot
    slot_rank = jnp.sum(earlier * one_hot, axis=1)
    target = flat_ids * capacity + slot_rank
    slot_ids = jnp.arange(slot_count, dtype=jnp.int32)
    placed = (target[None, :] == slot_ids[:, None]).reshape(slot_count, seq_count, top_count)
    dispatch_map = jnp.sum(placed.astype(jnp.float32), axis=2).astype(jnp.bfloat16)
    outgoing = jnp.dot(dispatch_map, rows_own, preferred_element_type=jnp.float32).astype(
        jnp.bfloat16
    )
    outgoing = outgoing.reshape(ep_count, expert_dev * capacity, slice_width)
    incoming = lax.all_to_all(outgoing, "ep", split_axis=0, concat_axis=0, tiled=True)
    arrived = incoming.reshape(ep_count, expert_dev, capacity, slice_width)
    gate_part = jnp.einsum(
        "secd,edf->secf", arrived, expert_gate, preferred_element_type=jnp.float32
    )
    up_part = jnp.einsum("secd,edf->secf", arrived, expert_up, preferred_element_type=jnp.float32)
    gate_full, up_full = (
        lax.psum(gate_part.astype(jnp.bfloat16), "tp").astype(jnp.float32),
        lax.psum(up_part.astype(jnp.bfloat16), "tp").astype(jnp.float32),
    )
    inner_rows = (jax.nn.silu(gate_full) * up_full).astype(jnp.bfloat16)
    expert_terms = jnp.einsum(
        "secf,efd->secd", inner_rows, expert_down, preferred_element_type=jnp.float32
    )
    returned = lax.all_to_all(
        expert_terms.reshape(ep_count, expert_dev * capacity, slice_width).astype(jnp.bfloat16),
        "ep",
        split_axis=0,
        concat_axis=0,
        tiled=True,
    ).astype(jnp.float32)
    weights = route_weight / jnp.sum(route_weight, axis=1, keepdims=True) * ROUTED_SCALE
    chosen = target.reshape(seq_count, top_count)[:, :, None] == slot_ids[None, None, :]
    combine = jnp.sum(jnp.where(chosen, weights[:, :, None], 0.0), axis=1)
    routed = jnp.dot(combine, returned.reshape(slot_count, slice_width), precision=HIGH)
    shared_gate_rows = jnp.dot(ffn_rows, shared_gate, preferred_element_type=jnp.float32)
    shared_up_rows = jnp.dot(ffn_rows, shared_up, preferred_element_type=jnp.float32)
    shared_inner = (jax.nn.silu(shared_gate_rows) * shared_up_rows).astype(jnp.bfloat16)
    shared_terms = jnp.dot(shared_inner, shared_down, preferred_element_type=jnp.float32)
    shared_own = lax.psum_scatter(
        shared_terms.astype(jnp.bfloat16), "tp", scatter_dimension=1, tiled=True
    ).astype(jnp.float32)
    mixed = (resid_own.astype(jnp.float32) + shared_own + routed).astype(jnp.bfloat16)
    return (mixed, new_real, new_imag)


def solution(mesh):
    placed = (
        P("ep", None),
        P(),
        P(),
        P(None, "tp"),
        P("tp"),
        P("tp"),
        P("tp"),
        P(None, "tp"),
        P(None, "tp"),
        P(None, "tp"),
        P(None, "tp"),
        P("tp"),
        P("ep", "tp"),
        P("ep", "tp"),
        P("tp", None),
        P(None, "tp"),
        P(None, "tp"),
        P("tp", None),
        P("ep", "tp", None),
        P("ep", "tp", None),
        P("ep", None, "tp"),
        P("ep", None),
        P("ep", None),
    )
    return jax.shard_map(
        local,
        mesh=mesh,
        in_specs=placed,
        out_specs=(P("ep", "tp"), P("ep", "tp"), P("ep", "tp")),
        check_vma=False,
    )
```

profile of v0, /device:TPU:0, one launch (start us, length us, event | category | flops | bytes accessed | tf_op | source)
XLA Modules:
  0.0 197.0 jit_solution(18267901409263895610)
XLA Ops:
  7.3 0.8 exp.27
  8.1 1.2 fusion.34
  9.4 0.8 reshape.245
  10.1 0.8 mul.328
  10.9 0.7 fusion.74
  11.7 2.3 %convolution_convert_fusion.2 = bf16[64,256]{1,0:T(8,128)(2,1)S(1)} fusion(bf16[4096,256]{1,0:T(8,128)(2,1)} %param.26, bf16[64,4096]{1,0:T(8,128)(2,1)} %param.23, f32[4096]{0:T(1024)} %param.24, f32[64]{0:T(128)S(1)} %add_rsqrt_fusion), kind=kOutput, calls=%fused_computation.28 | convolution fusion | flops 135282688 | bytes 2670848 | tf_op jit(solution)/shard_map/dot_general | solution.py:35
  14.4 0.7 reshape.251
  15.2 1.0 reshape.246
  16.1 0.9 reshape.247
  17.6 1.9 bitcast_add_fusion
  19.6 0.9 fusion.55
  20.5 1.0 fusion.50
  21.5 1.5 fusion.75
  24.6 0.8 dynamic_slice.7
  25.5 33.1 %reduce-scatter.3.cloned.1.call-done = f32[64,512]{1,0:T(8,128)} async-done(((f32[64,4096]{1,0:T(8,128)}), f32[64,512]{1,0:T(8,128)}) %reduce-scatter.3.cloned.1.call-update) | async-done | bytes 131088 | tf_op jit(solution)/shard_map/reduce_scatter | solution.py:116
  58.5 1.0 fusion.51
  59.6 13.9 %psum.21 = f32[64,1]{0,1:T(1,128)S(1)} all-reduce(f32[64,1]{0,1:T(1,128)S(1)} %bitcast.105), channel_id=1, replica_groups=mesh['ep'=4,'tp'=8] {'tp'}, use_global_device_ids=true, to_apply=%region_3.0 | all-reduce | flops 64 | bytes 512 | tf_op jit(solution)/shard_map/psum | solution.py:120
  73.9 11.7 %all_to_all.10 = bf16[4,128,512]{2,1,0:T(8,128)(2,1)S(1)} all-to-all(bf16[4,128,512]{2,1,0:T(8,128)(2,1)S(1)} %bitcast.99), channel_id=1, replica_groups=mesh['ep'=4,'tp'=8] {'ep'}, dimensions={0} | all-to-all | bytes 1048576 | tf_op jit(solution)/shard_map/all_to_all | solution.py:144
  85.6 4.0 %fusion.17 = bf16[4,4,32,1024]{3,2,0,1:T(8,128)(2,1)} fusion(bf16[4,512,1024]{2,1,0:T(8,128)(2,1)} %param.42, bf16[4,4,32,512]{3,2,1,0:T(8,128)(2,1)S(1)} %bitcast.97), kind=kOutput, calls=%fused_computation.16 | convolution fusion | flops 537395200 | bytes 5767168 | tf_op jit(solution)/shard_map/secd,edf->secf/dot_general | solution.py:149
  89.6 1.7 fusion.20
  91.4 16.5 %all_gather.3 = bf16[64,4096]{1,0:T(8,128)(2,1)S(1)} all-gather(bf16[64,512]{1,0:T(8,128)(2,1)S(1)} %fusion.53), channel_id=1, replica_groups=mesh['ep'=4,'tp'=8] {'tp'}, dimensions={1}, use_global_device_ids=true | all-gather | bytes 589824 | tf_op jit(solution)/shard_map/all_gather | solution.py:124
  107.9 1.5 fusion.76
  109.5 3.0 %convolution_convert_fusion = bf16[64,4096]{1,0:T(8,128)(2,1)} fusion(bf16[128,4096]{1,0:T(8,128)(2,1)} %param.40, bf16[64,4096]{1,0:T(8,128)(2,1)S(1)} %all_gather.3, bf16[4096,128]{1,0:T(8,128)(2,1)} %param.39, f32[64,128]{1,0:T(8,128)S(1)} %fusion.76), kind=kOutput, calls=%fused_computation | convolution fusion | flops 134529024 | bytes 3178496 | tf_op jit(solution)/shard_map/dot_general | solution.py:172
  112.5 42.7 %all-reduce.3.cloned.1.call-done = (bf16[4,4,32,1024]{3,2,0,1:T(8,128)(2,1)}, bf16[4,4,32,1024]{3,2,0,1:T(8,128)(2,1)}) async-done(((bf16[4,4,32,1024]{3,2,0,1:T(8,128)(2,1)}, bf16[4,4,32,1024]{3,2,0,1:T(8,128)(2,1)}), (bf16[4,4,32,1024]{3,2,0,1:T(8,128)(2,1)}, bf16[4,4,32,1024]{3,2,0,1:T(8,128)(2,1)})) %all-reduce.3.cloned.1.call-update) | async-done | bytes 2097168 | tf_op jit(solution)/shard_map/psum | solution.py:152
  155.1 3.7 %fusion.26 = bf16[4,4,32,512]{3,2,0,1:T(8,128)(2,1)S(1)} fusion(bf16[4,1024,512]{2,1,0:T(8,128)(2,1)} %param.43, bf16[4,4,32,1024]{3,2,0,1:T(8,128)(2,1)} %get-tuple-element.3, bf16[4,4,32,1024]{3,2,0,1:T(8,128)(2,1)} %get-tuple-element.4), kind=kOutput, calls=%fused_computation.22 | convolution fusion | flops 541327360 | bytes 6815744 | tf_op jit(solution)/shard_map/secf,efd->secd/dot_general | solution.py:155
  158.9 0.9 copy.91
  159.7 4.1 %all-to-all-start.1 = ((bf16[4,128,512]{2,1,0:T(8,128)(2,1)}), bf16[4,128,512]{2,1,0:T(8,128)(2,1)}, u32[]{:S(2)}, u32[]{:S(2)}) async-start(bf16[4,128,512]{2,1,0:T(8,128)(2,1)} %bitcast.100), calls=%async_computation.3 | async-start | bytes 1048576 | tf_op jit(solution)/shard_map/all_to_all | solution.py:158
  163.9 1.1 copy.93
  165.3 1.9 reshape.259
  167.2 0.9 reshape.258
  168.3 20.2 %reduce-scatter.5.cloned.1.call-done = bf16[64,512]{1,0:T(8,128)(2,1)} async-done(((bf16[64,4096]{1,0:T(8,128)(2,1)}), bf16[64,512]{1,0:T(8,128)(2,1)}) %reduce-scatter.5.cloned.1.call-update) | async-done | bytes 65552 | tf_op jit(solution)/shard_map/reduce_scatter | solution.py:173
  188.4 2.1 %fusion.31 = bf16[64,512]{1,0:T(8,128)(2,1)} fusion(f32[64,512]{1,0:T(8,128)S(1)} %select_reduce_fusion, bf16[512,512]{1,0:T(8,128)(2,1)} %bitcast.22, bf16[64,512]{1,0:T(8,128)(2,1)S(1)} %get-tuple-element.6, bf16[64,512]{1,0:T(8,128)(2,1)} %reduce-scatter.5.cloned.1.call-done), kind=kOutput, calls=%fused_computation.27 | convolution fusion | flops 201490432 | bytes 851968 | tf_op jit(solution)/shard_map/dot_general | solution.py:168
  (62 shorter events, 3.7 us)
Async XLA Ops:
  7.2 14.4 %copy-start = (bf16[256,4096]{1,0:T(8,128)(2,1)S(1)}, bf16[256,4096]{1,0:T(8,128)(2,1)}, u32[]{:S(2)}) copy-start(bf16[256,4096]{1,0:T(8,128)(2,1)} %param.37) | copy-start | bytes 6291460
  7.2 7.0 %copy-start.7 = (f32[16,1024]{1,0:T(8,128)S(1)}, f32[16,1024]{1,0:T(8,128)}, u32[]{:S(2)}) copy-start(f32[16,1024]{1,0:T(8,128)} %param.30) | copy-start | bytes 196612
  7.2 7.1 %copy-start.8 = (f32[16,1024]{1,0:T(8,128)S(1)}, f32[16,1024]{1,0:T(8,128)}, u32[]{:S(2)}) copy-start(f32[16,1024]{1,0:T(8,128)} %param.31) | copy-start | bytes 196612
  7.2 7.2 %copy-start.9 = (f32[16,1024]{1,0:T(8,128)S(1)}, f32[16,1024]{1,0:T(8,128)}, u32[]{:S(2)}) copy-start(f32[16,1024]{1,0:T(8,128)} %param.32) | copy-start | bytes 196612
  7.2 7.9 %copy-start.10 = (f32[16,1024]{1,0:T(8,128)S(1)}, f32[16,1024]{1,0:T(8,128)}, u32[]{:S(2)}) copy-start(f32[16,1024]{1,0:T(8,128)} %param.33) | copy-start | bytes 196612
  7.2 8.0 %copy-start.5 = (f32[64,1024]{1,0:T(8,128)S(1)}, f32[64,1024]{1,0:T(8,128)}, u32[]{:S(2)}) copy-start(f32[64,1024]{1,0:T(8,128)} %param.35) | copy-start | bytes 786436
  7.2 51.3 %reduce-scatter.3.cloned.1.call-start = ((), (), s32[]{:S(2)}) async-start(), calls=%async_computation.4 | async-start | bytes 1179648 | tf_op jit(solution)/shard_map/reduce_scatter | solution.py:116
  11.7 4.4 %copy-start.6 = (f32[64,1024]{1,0:T(8,128)S(1)}, f32[64,1024]{1,0:T(8,128)}, u32[]{:S(2)}) copy-start(f32[64,1024]{1,0:T(8,128)} %param.36) | copy-start | bytes 786436
  17.1 2.5 %copy-start.4 = (f32[16,16,64]{2,1,0:T(8,128)S(1)}, f32[16,16,64]{2,1,0:T(8,128)}, u32[]{:S(2)}) copy-start(f32[16,16,64]{2,1,0:T(8,128)} %reshape.251) | copy-start | bytes 196612
  19.6 3.5 %copy-start.1 = (f32[64,16,64]{2,0,1:T(8,128)}, f32[64,16,64]{2,0,1:T(8,128)S(1)}, u32[]{:S(2)}) copy-start(f32[64,16,64]{2,0,1:T(8,128)S(1)} %get-tuple-element.7) | copy-start | bytes 786436
  21.5 1.6 copy-start.11
  23.1 132.1 %all-reduce.3.cloned.1.call-start = ((), (), s32[]{:S(2)}) async-start(), calls=%async_computation.6 | async-start | bytes 4194304 | tf_op jit(solution)/shard_map/psum | solution.py:152
  85.6 4.0 %copy-start.3 = (bf16[4,512,1024]{2,1,0:T(8,128)(2,1)S(1)}, bf16[4,512,1024]{2,1,0:T(8,128)(2,1)}, u32[]{:S(2)}) copy-start(bf16[4,512,1024]{2,1,0:T(8,128)(2,1)} %param.41) | copy-start | bytes 12582916
  91.4 97.0 %reduce-scatter.5.cloned.1.call-start = ((), (), s32[]{:S(2)}) async-start(), calls=%async_computation.5 | async-start | bytes 589824 | tf_op jit(solution)/shard_map/reduce_scatter | solution.py:173
  158.8 5.0 %copy-start.2 = (f32[64,16,64]{2,0,1:T(8,128)S(1)}, f32[64,16,64]{2,0,1:T(8,128)}, u32[]{:S(2)}) copy-start(f32[64,16,64]{2,0,1:T(8,128)} %copy-done.1) | copy-start | bytes 786436
  159.7 28.7 %all-to-all-start.1 = ((bf16[4,128,512]{2,1,0:T(8,128)(2,1)}), bf16[4,128,512]{2,1,0:T(8,128)(2,1)}, u32[]{:S(2)}, u32[]{:S(2)}) async-start(bf16[4,128,512]{2,1,0:T(8,128)(2,1)} %bitcast.100), calls=%async_computation.3 | async-start | bytes 1048576 | tf_op jit(solution)/shard_map/all_to_all | solution.py:158
  163.9 4.2 %copy-start.12 = (f32[64,4]{0,1:T(4,128)S(1)}, f32[64,4]{0,1:T(4,128)}, u32[]{:S(2)}) copy-start(f32[64,4]{0,1:T(4,128)} %param.45) | copy-start | bytes 3076
Sparse Core Ops, SparseCore 0:
  23.2 35.2 reduce-scatter.2
  91.5 63.6 all-reduce.2
  157.4 30.9 reduce-scatter.4
where the time goes:
time: 198 us; the launch traced here: 197 us
  waiting for transfers between devices  96 us (48%)
  blocking collectives  42.1 us (21%)
  matrix products  24.4 us (12%)
  between operations  14 us (7%)
  local copies, waits for them, and re-layouts  12 us (6%)
  starting transfers between devices  4.25 us (2%)
  other arithmetic  4.21 us (2%)
    psum x1, waiting for transfers between devices, local(): lax.psum(up_part.astype(jnp.bfloat16), 'tp').astype(jnp.float32)  42.7 us
    reduce_scatter x1, waiting for transfers between devices, local(): lax.psum_scatter(mixer_terms, 'tp', scatter_dimension=1, tiled=True)  33.1 us
    reduce_scatter x1, waiting for transfers between devices, local(): lax.psum_scatter(shared_terms.astype(jnp.bfloat16), 'tp', scatter_dimensi...  20.2 us
    all_gather x1, blocking collectives, local(): ffn_rows = lax.all_gather(rows_own, 'tp', axis=1, tiled=True)  16.5 us
    psum x1, blocking collectives, local(): lax.psum(jnp.sum(resid_f * resid_f, axis=1, keepdims=True), 'tp')  13.9 us
    all_to_all x1, blocking collectives, local(): lax.all_to_all(outgoing, 'ep', split_axis=0, concat_axis=0, tiled=True)  11.7 us
    all_to_all x1, starting transfers between devices, local(): lax.all_to_all(expert_terms.reshape(ep_count, expert_dev * capacity, slic...  4.13 us
    dot_general x1, matrix products, local(): jnp.einsum('secd,edf->secf', arrived, expert_up, preferred_element_type=j...  4.04 us
  transfers between devices with their start and end apart: 4, of which 3 were waited for; matrix products, arithmetic and copies ran while one was open for 8% of the time, Pallas kernels for 0%

commit v1 on v0

--- a/solution.py
+++ b/solution.py
@@ -1,3 +1,4 @@
+import functools
 import jax
 import jax.numpy as jnp
 from jax import lax
@@ -6,6 +7,19 @@
 EPS = 1e-06
 ROUTED_SCALE = 2.5
 HIGH = lax.Precision.HIGHEST
+
+
+def meet_chunk(field, axis_name):
+    before = jnp.concatenate(
+        lax.all_to_all(
+            jnp.stack([field for _ in range(lax.axis_size(axis_name))], 0), axis_name, 0, 0
+        ),
+        1,
+    )
+    return before
+
+
+goods_convert = functools.partial(meet_chunk, axis_name="tp")
 
 
 def rms_scale(values_in, gains):
@@ -121,7 +135,7 @@
     factor = lax.rsqrt(square_sum / model_width + EPS)
     gain_own = lax.dynamic_slice_in_dim(ffn_gain, offset, slice_width, 0)
     rows_own = (resid_f * factor * gain_own).astype(jnp.bfloat16)
-    ffn_rows = lax.all_gather(rows_own, "tp", axis=1, tiled=True)
+    ffn_rows = goods_convert(rows_own)
     expert_dev = expert_gate.shape[0]
     expert_count = expert_dev * ep_count
     top_count = routing.shape[1]

time: 198 us -> 204 us (1.030)
  waiting for transfers between devices: 96 us -> 113 us
  blocking collectives: 42.1 us -> 25.6 us
  starting transfers between devices: 4.25 us -> 8.39 us
    all_gather x1 -> x0, blocking collectives: 16.5 us -> none  [local(): ffn_rows = lax.all_gather(rows_own, 'tp', axis=1, tiled=True)]
    all_to_all x0 -> x1, waiting for transfers between devices: none -> 11.1 us  [meet_chunk(): lax.all_to_all(jnp.stack([field for _ in range(lax.axis_size(axis_name))]...]
    psum x1, waiting for transfers between devices: 42.7 us -> 48.3 us  [local(): lax.psum(up_part.astype(jnp.bfloat16), 'tp').astype(jnp.float32)]
    all_to_all x0 -> x1, starting transfers between devices: none -> 4.14 us  [meet_chunk(): lax.all_to_all(jnp.stack([field for _ in range(lax.axis_size(axis_name))]...]
    reduce_scatter x1, waiting for transfers between devices: 20.2 us -> 17.5 us  [local(): lax.psum_scatter(shared_terms.astype(jnp.bfloat16), 'tp', scatter_dimensi...]
    all_to_all x1, waiting for transfers between devices: 0.01 us -> 2.63 us  [local(): lax.all_to_all(expert_terms.reshape(ep_count, expert_dev * capacity, slic...]
  transfers between devices with their start and end apart: 4 -> 5, of which waited for: 3 -> 5; matrix products, arithmetic and copies ran while one was open for 8% -> 11% of each run, Pallas kernels for 0% -> 0%
where the time goes in v1:
time: 204 us; the launch traced here: 203 us
  waiting for transfers between devices  113 us (55%)
  blocking collectives  25.6 us (13%)
  matrix products  24.4 us (12%)
  local copies, waits for them, and re-layouts  14 us (7%)
  between operations  14 us (7%)
  starting transfers between devices  8.39 us (4%)
  other arithmetic  4.21 us (2%)
    psum x1, waiting for transfers between devices, local(): lax.psum(up_part.astype(jnp.bfloat16), 'tp').astype(jnp.float32)  48.3 us
    reduce_scatter x1, waiting for transfers between devices, local(): lax.psum_scatter(mixer_terms, 'tp', scatter_dimension=1, tiled=True)  33.1 us
    reduce_scatter x1, waiting for transfers between devices, local(): lax.psum_scatter(shared_terms.astype(jnp.bfloat16), 'tp', scatter_dimensi...  17.5 us
    psum x1, blocking collectives, local(): lax.psum(jnp.sum(resid_f * resid_f, axis=1, keepdims=True), 'tp')  13.9 us
    all_to_all x1, blocking collectives, local(): lax.all_to_all(outgoing, 'ep', split_axis=0, concat_axis=0, tiled=True)  11.7 us
    all_to_all x1, waiting for transfers between devices, meet_chunk(): lax.all_to_all(jnp.stack([field for _ in range(lax.axis_size(axis_name))]...  11.1 us
    all_to_all x1, starting transfers between devices, meet_chunk(): lax.all_to_all(jnp.stack([field for _ in range(lax.axis_size(axis_name))]...  4.14 us
    all_to_all x1, starting transfers between devices, local(): lax.all_to_all(expert_terms.reshape(ep_count, expert_dev * capacity, slic...  4.13 us
  transfers between devices with their start and end apart: 5, of which 5 were waited for; matrix products, arithmetic and copies ran while one was open for 11% of the time, Pallas kernels for 0%

profile of v1, /device:TPU:0, one launch (start us, length us, event | category | flops | bytes accessed | tf_op | source)
XLA Modules:
  0.0 203.4 jit_solution(6306441812614576240)
XLA Ops:
  7.3 0.8 exp.27
  8.1 1.2 fusion.34
  11.7 2.3 %convolution_convert_fusion.2 = bf16[64,256]{1,0:T(8,128)(2,1)S(1)} fusion(bf16[4096,256]{1,0:T(8,128)(2,1)} %param.26, bf16[64,4096]{1,0:T(8,128)(2,1)} %param.23, f32[4096]{0:T(1024)} %param.24, f32[64]{0:T(128)S(1)} %add_rsqrt_fusion), kind=kOutput, calls=%fused_computation.28 | convolution fusion | flops 135282688 | bytes 2670848 | tf_op jit(solution)/shard_map/dot_general | solution.py:49
  15.2 1.0 reshape.254
  16.1 0.9 reshape.255
  17.6 1.9 bitcast_add_fusion
  19.6 0.9 fusion.55
  20.5 1.0 fusion.50
  21.5 1.5 fusion.75
  24.5 0.8 dynamic_slice.7
  25.4 33.1 %reduce-scatter.3.cloned.1.call-done = f32[64,512]{1,0:T(8,128)} async-done(((f32[64,4096]{1,0:T(8,128)}), f32[64,512]{1,0:T(8,128)}) %reduce-scatter.3.cloned.1.call-update) | async-done | bytes 131088 | tf_op jit(solution)/shard_map/reduce_scatter | solution.py:130
  58.5 1.0 fusion.51
  59.6 13.9 %psum.21 = f32[64,1]{0,1:T(1,128)S(1)} all-reduce(f32[64,1]{0,1:T(1,128)S(1)} %bitcast.110), channel_id=1, replica_groups=mesh['ep'=4,'tp'=8] {'tp'}, use_global_device_ids=true, to_apply=%region_3.0 | all-reduce | flops 64 | bytes 512 | tf_op jit(solution)/shard_map/psum | solution.py:134
  73.9 11.7 %all_to_all.15 = bf16[4,128,512]{2,1,0:T(8,128)(2,1)S(1)} all-to-all(bf16[4,128,512]{2,1,0:T(8,128)(2,1)S(1)} %bitcast.104), channel_id=1, replica_groups=mesh['ep'=4,'tp'=8] {'ep'}, dimensions={0} | all-to-all | bytes 1048576 | tf_op jit(solution)/shard_map/all_to_all | solution.py:158
  85.6 0.8 stack.2
  86.4 4.1 %all-to-all-start = ((bf16[8,64,512]{2,1,0:T(8,128)(2,1)}), bf16[8,64,512]{2,1,0:T(8,128)(2,1)}, u32[]{:S(2)}, u32[]{:S(2)}) async-start(bf16[8,64,512]{2,1,0:T(8,128)(2,1)} %stack.2), calls=%async_computation.1 | async-start | bytes 1048576 | tf_op jit(solution)/shard_map/all_to_all | solution.py:14
  90.7 4.0 %fusion.17 = bf16[4,4,32,1024]{3,2,0,1:T(8,128)(2,1)} fusion(bf16[4,512,1024]{2,1,0:T(8,128)(2,1)} %param.42, bf16[4,4,32,512]{3,2,1,0:T(8,128)(2,1)S(1)} %bitcast.102), kind=kOutput, calls=%fused_computation.16 | convolution fusion | flops 537395200 | bytes 5767168 | tf_op jit(solution)/shard_map/secd,edf->secf/dot_general | solution.py:163
  94.7 1.7 fusion.20
  96.5 11.1 %all-to-all-done = bf16[8,64,512]{2,1,0:T(8,128)(2,1)} async-done(((bf16[8,64,512]{2,1,0:T(8,128)(2,1)}), bf16[8,64,512]{2,1,0:T(8,128)(2,1)}, u32[]{:S(2)}, u32[]{:S(2)}) %all-to-all-start) | async-done | bytes 524320 | tf_op jit(solution)/shard_map/all_to_all | solution.py:14
  107.6 1.1 copy.120
  108.7 1.6 fusion.76
  110.2 3.0 %convolution_convert_fusion = bf16[64,4096]{1,0:T(8,128)(2,1)} fusion(bf16[128,4096]{1,0:T(8,128)(2,1)} %param.40, bf16[64,4096]{1,0:T(8,128)(2,1)S(1)} %bitcast.101, bf16[4096,128]{1,0:T(8,128)(2,1)} %param.39, f32[64,128]{1,0:T(8,128)S(1)} %fusion.76), kind=kOutput, calls=%fused_computation | convolution fusion | flops 134529024 | bytes 3178496 | tf_op jit(solution)/shard_map/dot_general | solution.py:186
  113.2 48.3 %all-reduce.3.cloned.1.call-done = (bf16[4,4,32,1024]{3,2,0,1:T(8,128)(2,1)}, bf16[4,4,32,1024]{3,2,0,1:T(8,128)(2,1)}) async-done(((bf16[4,4,32,1024]{3,2,0,1:T(8,128)(2,1)}, bf16[4,4,32,1024]{3,2,0,1:T(8,128)(2,1)}), (bf16[4,4,32,1024]{3,2,0,1:T(8,128)(2,1)}, bf16[4,4,32,1024]{3,2,0,1:T(8,128)(2,1)})) %all-reduce.3.cloned.1.call-update) | async-done | bytes 2097168 | tf_op jit(solution)/shard_map/psum | solution.py:166
  161.6 3.7 %fusion.26 = bf16[4,4,32,512]{3,2,0,1:T(8,128)(2,1)S(1)} fusion(bf16[4,1024,512]{2,1,0:T(8,128)(2,1)} %param.43, bf16[4,4,32,1024]{3,2,0,1:T(8,128)(2,1)} %get-tuple-element.3, bf16[4,4,32,1024]{3,2,0,1:T(8,128)(2,1)} %get-tuple-element.4), kind=kOutput, calls=%fused_computation.22 | convolution fusion | flops 541327360 | bytes 6815744 | tf_op jit(solution)/shard_map/secf,efd->secd/dot_general | solution.py:169
  165.3 0.9 copy.114
  166.1 4.1 %all-to-all-start.2 = ((bf16[4,128,512]{2,1,0:T(8,128)(2,1)}), bf16[4,128,512]{2,1,0:T(8,128)(2,1)}, u32[]{:S(2)}, u32[]{:S(2)}) async-start(bf16[4,128,512]{2,1,0:T(8,128)(2,1)} %bitcast.105), calls=%async_computation.4 | async-start | bytes 1048576 | tf_op jit(solution)/shard_map/all_to_all | solution.py:172
  170.3 1.1 copy.116
  171.7 1.9 reshape.269
  173.6 0.9 reshape.268
  174.7 2.6 %all-to-all-done.2 = bf16[4,128,512]{2,1,0:T(8,128)(2,1)} async-done(((bf16[4,128,512]{2,1,0:T(8,128)(2,1)}), bf16[4,128,512]{2,1,0:T(8,128)(2,1)}, u32[]{:S(2)}, u32[]{:S(2)}) %all-to-all-start.2) | async-done | bytes 524320 | tf_op jit(solution)/shard_map/all_to_all | solution.py:172
  177.3 17.5 %reduce-scatter.5.cloned.1.call-done = bf16[64,512]{1,0:T(8,128)(2,1)} async-done(((bf16[64,4096]{1,0:T(8,128)(2,1)}), bf16[64,512]{1,0:T(8,128)(2,1)}) %reduce-scatter.5.cloned.1.call-update) | async-done | bytes 65552 | tf_op jit(solution)/shard_map/reduce_scatter | solution.py:187
  194.8 2.1 %fusion.31 = bf16[64,512]{1,0:T(8,128)(2,1)} fusion(f32[64,512]{1,0:T(8,128)S(1)} %select_reduce_fusion, bf16[512,512]{1,0:T(8,128)(2,1)} %bitcast.23, bf16[64,512]{1,0:T(8,128)(2,1)S(1)} %get-tuple-element.6, bf16[64,512]{1,0:T(8,128)(2,1)} %reduce-scatter.5.cloned.1.call-done), kind=kOutput, calls=%fused_computation.27 | convolution fusion | flops 201490432 | bytes 851968 | tf_op jit(solution)/shard_map/dot_general | solution.py:182
  (65 shorter events, 6.7 us)
Async XLA Ops:
  7.2 14.4 %copy-start = (bf16[256,4096]{1,0:T(8,128)(2,1)S(1)}, bf16[256,4096]{1,0:T(8,128)(2,1)}, u32[]{:S(2)}) copy-start(bf16[256,4096]{1,0:T(8,128)(2,1)} %param.37) | copy-start | bytes 6291460
  7.2 7.0 %copy-start.7 = (f32[16,1024]{1,0:T(8,128)S(1)}, f32[16,1024]{1,0:T(8,128)}, u32[]{:S(2)}) copy-start(f32[16,1024]{1,0:T(8,128)} %param.30) | copy-start | bytes 196612
  7.2 7.1 %copy-start.8 = (f32[16,1024]{1,0:T(8,128)S(1)}, f32[16,1024]{1,0:T(8,128)}, u32[]{:S(2)}) copy-start(f32[16,1024]{1,0:T(8,128)} %param.31) | copy-start | bytes 196612
  7.2 7.2 %copy-start.9 = (f32[16,1024]{1,0:T(8,128)S(1)}, f32[16,1024]{1,0:T(8,128)}, u32[]{:S(2)}) copy-start(f32[16,1024]{1,0:T(8,128)} %param.32) | copy-start | bytes 196612
  7.2 7.9 %copy-start.10 = (f32[16,1024]{1,0:T(8,128)S(1)}, f32[16,1024]{1,0:T(8,128)}, u32[]{:S(2)}) copy-start(f32[16,1024]{1,0:T(8,128)} %param.33) | copy-start | bytes 196612
  7.2 8.0 %copy-start.5 = (f32[64,1024]{1,0:T(8,128)S(1)}, f32[64,1024]{1,0:T(8,128)}, u32[]{:S(2)}) copy-start(f32[64,1024]{1,0:T(8,128)} %param.35) | copy-start | bytes 786436
  7.2 51.3 %reduce-scatter.3.cloned.1.call-start = ((), (), s32[]{:S(2)}) async-start(), calls=%async_computation.5 | async-start | bytes 1179648 | tf_op jit(solution)/shard_map/reduce_scatter | solution.py:130
  11.7 4.4 %copy-start.6 = (f32[64,1024]{1,0:T(8,128)S(1)}, f32[64,1024]{1,0:T(8,128)}, u32[]{:S(2)}) copy-start(f32[64,1024]{1,0:T(8,128)} %param.36) | copy-start | bytes 786436
  17.1 2.5 %copy-start.4 = (f32[16,16,64]{2,1,0:T(8,128)S(1)}, f32[16,16,64]{2,1,0:T(8,128)}, u32[]{:S(2)}) copy-start(f32[16,16,64]{2,1,0:T(8,128)} %reshape.259) | copy-start | bytes 196612
  19.6 3.5 %copy-start.1 = (f32[64,16,64]{2,0,1:T(8,128)}, f32[64,16,64]{2,0,1:T(8,128)S(1)}, u32[]{:S(2)}) copy-start(f32[64,16,64]{2,0,1:T(8,128)S(1)} %get-tuple-element.7) | copy-start | bytes 786436
  21.5 1.5 copy-start.11
  86.4 21.2 %all-to-all-start = ((bf16[8,64,512]{2,1,0:T(8,128)(2,1)}), bf16[8,64,512]{2,1,0:T(8,128)(2,1)}, u32[]{:S(2)}, u32[]{:S(2)}) async-start(bf16[8,64,512]{2,1,0:T(8,128)(2,1)} %stack.2), calls=%async_computation.1 | async-start | bytes 1048576 | tf_op jit(solution)/shard_map/all_to_all | solution.py:14
  90.6 71.0 %all-reduce.3.cloned.1.call-start = ((), (), s32[]{:S(2)}) async-start(), calls=%async_computation.7 | async-start | bytes 4194304 | tf_op jit(solution)/shard_map/psum | solution.py:166
  90.6 4.1 %copy-start.3 = (bf16[4,512,1024]{2,1,0:T(8,128)(2,1)S(1)}, bf16[4,512,1024]{2,1,0:T(8,128)(2,1)}, u32[]{:S(2)}) copy-start(bf16[4,512,1024]{2,1,0:T(8,128)(2,1)} %param.41) | copy-start | bytes 12582916
  96.4 98.4 %reduce-scatter.5.cloned.1.call-start = ((), (), s32[]{:S(2)}) async-start(), calls=%async_computation.6 | async-start | bytes 589824 | tf_op jit(solution)/shard_map/reduce_scatter | solution.py:187
  165.3 5.0 %copy-start.2 = (f32[64,16,64]{2,0,1:T(8,128)S(1)}, f32[64,16,64]{2,0,1:T(8,128)}, u32[]{:S(2)}) copy-start(f32[64,16,64]{2,0,1:T(8,128)} %copy-done.1) | copy-start | bytes 786436
  166.1 11.2 %all-to-all-start.2 = ((bf16[4,128,512]{2,1,0:T(8,128)(2,1)}), bf16[4,128,512]{2,1,0:T(8,128)(2,1)}, u32[]{:S(2)}, u32[]{:S(2)}) async-start(bf16[4,128,512]{2,1,0:T(8,128)(2,1)} %bitcast.105), calls=%async_computation.4 | async-start | bytes 1048576 | tf_op jit(solution)/shard_map/all_to_all | solution.py:172
  170.3 4.2 %copy-start.12 = (f32[64,4]{0,1:T(4,128)S(1)}, f32[64,4]{0,1:T(4,128)}, u32[]{:S(2)}) copy-start(f32[64,4]{0,1:T(4,128)} %param.45) | copy-start | bytes 3076
Sparse Core Ops, SparseCore 0:
  23.2 35.2 reduce-scatter.2
  96.5 64.9 all-reduce.2
  163.8 30.9 reduce-scatter.4
